TPU v7x, 32 devices: a whole 2x2x4 slice. The times are simulated.
32 devices in a mesh: ep: 4 (over y, x), tp: 8 (over z, core).
Axes of the slice: x: 2, y: 2, z: 4, core: 2. Of those that a mesh axis runs over, the one named last changes fastest.
Arguments:
- pool_input: bfloat16 [4096, 1024], P('ep', 'tp'), may hold values from -6 to 6
- pool_gain: float32 [1024], P('tp'), may hold values from 0.1 to 1.9
- mix_weight: bfloat16 [1024, 2048], P('tp'), may hold values from -0.1875 to 0.1875
- moe_input: bfloat16 [8192, 2048], P(('ep', 'tp')), may hold values from -6 to 6
- moe_gain: float32 [2048], replicated, may hold values from 0.1 to 1.9
- expert_ids: int32 [8192, 2], P(('ep', 'tp')), may hold values from 0 to 15, as said below
- route_weight: float32 [8192, 2], P(('ep', 'tp')), may hold values from 0.2 to 1
- gate_weight: bfloat16 [16, 2048, 1024], P('ep', None, 'tp'), may hold values from -0.125 to 0.125
- up_weight: bfloat16 [16, 2048, 1024], P('ep', None, 'tp'), may hold values from -0.125 to 0.125
- down_weight: bfloat16 [16, 2048, 1024], P('ep', None, 'tp'), may hold values from -0.1875 to 0.1875
Outputs:
- mixed_out: bfloat16 [4096, 2048], P(('ep', 'tp'))
- moe_out: bfloat16 [8192, 2048], P(('ep', 'tp'))
Inputs may be any that keep to these rules, and one draw needn't show every extreme that they name: `expert_ids`: each row names 2 different experts of one group of 4 consecutive experts. In each aligned block of 256 rows (the rows of one device) no expert is named by more than 48 rows, and some expert is named by exactly 48 rows.
All inputs are finite; a program needn't handle non-finite values.
Results may differ from a plain program's by a relative error of at most 0.012.
Values may be sent and summed in bfloat16 or wider, within the bound.
A program may use at most 128 MiB of HBM per device.

v0:
```python
import jax
import jax.numpy as jnp
from jax import lax
from jax.sharding import PartitionSpec as P

GROUP_CH = 256
EXPERTS = 16
TOP = 2
CAP = 48
eps_norm = 1e-06


def from_behind(shard, axis, by):
    peers = lax.axis_size(axis)
    pairs = [(i, i + by) for i in range(peers) if 0 <= i + by < peers]
    return lax.ppermute(shard, axis, pairs)


def window_sums(extended, row_count):
    level_sum = extended
    stride = 1
    outputs = []
    for doubling in range(4):
        level_sum = level_sum[stride:] + level_sum[:-stride]
        stride = stride * 2
        outputs.append(level_sum[level_sum.shape[0] - row_count :])
    return outputs


def pool_mixer(pool_input, pool_gain):
    row_count, channels = pool_input.shape
    carried = from_behind(pool_input[row_count - 15 :], "ep", 1)
    extended = jnp.concatenate([carried, pool_input], axis=0).astype(jnp.float32)
    window_list = window_sums(extended, row_count)
    channel_ids = lax.axis_index("tp") * channels + lax.iota(jnp.int32, channels)
    group_ids = channel_ids // GROUP_CH
    position = lax.axis_index("ep") * row_count + lax.iota(jnp.int32, row_count)
    summed = jnp.zeros((row_count, channels), jnp.float32)
    widths = jnp.zeros((channels,), jnp.int32)
    for index_group in range(4):
        inside = group_ids == index_group
        summed = jnp.where(inside[None, :], window_list[index_group], summed)
        widths = jnp.where(inside, 2 ** (index_group + 1), widths)
    counted = jnp.minimum(position[:, None] + 1, widths[None, :]).astype(jnp.float32)
    values = extended[15:]
    return ((summed / counted - values) * pool_gain).astype(jnp.bfloat16)


def route_slots(expert_ids):
    flat_ids = expert_ids.reshape(-1)
    marked = (flat_ids[:, None] == lax.iota(jnp.int32, EXPERTS)[None, :]).astype(jnp.int32)
    before_count = jnp.cumsum(marked, axis=0) - marked
    ranked = jnp.sum(before_count * marked, axis=1)
    return (flat_ids * CAP + ranked).reshape(expert_ids.shape)


def body(
    pool_input,
    pool_gain,
    mix_weight,
    moe_input,
    moe_gain,
    expert_ids,
    route_weight,
    gate_weight,
    up_weight,
    down_weight,
):
    pooled = pool_mixer(pool_input, pool_gain)
    regrouped = lax.all_to_all(pooled, "tp", split_axis=0, concat_axis=1, tiled=True)
    mixed_sum = jnp.dot(
        regrouped,
        lax.all_gather(mix_weight, "tp", axis=0, tiled=True),
        preferred_element_type=jnp.float32,
    )
    mixed_out = mixed_sum.astype(jnp.bfloat16)
    inputs = moe_input.astype(jnp.float32)
    scale_rows = lax.rsqrt(jnp.mean(inputs * inputs, axis=-1, keepdims=True) + eps_norm)
    normed = (inputs * scale_rows * moe_gain).astype(jnp.bfloat16)
    slots = route_slots(expert_ids)
    slot_index = lax.iota(jnp.int32, EXPERTS * CAP)
    placing = (
        (slot_index[:, None] == slots[None, :, 0]) | (slot_index[:, None] == slots[None, :, 1])
    ).astype(jnp.bfloat16)
    outgoing = jnp.dot(placing, normed, preferred_element_type=jnp.float32).astype(jnp.bfloat16)
    outgoing = outgoing.reshape(EXPERTS, CAP, normed.shape[1])
    arrived = lax.all_to_all(outgoing, "ep", split_axis=0, concat_axis=1, tiled=True)
    gate_piece = lax.all_gather(gate_weight, "tp", axis=2, tiled=True)
    up_piece = lax.all_gather(up_weight, "tp", axis=2, tiled=True)
    down_piece = lax.all_gather(down_weight, "tp", axis=2, tiled=True)
    gate_part = jnp.einsum("erd,edf->erf", arrived, gate_piece, preferred_element_type=jnp.float32)
    upward = jnp.einsum("erd,edf->erf", arrived, up_piece, preferred_element_type=jnp.float32)
    hidden = (jax.nn.silu(gate_part) * upward).astype(jnp.bfloat16)
    expert_sum = jnp.einsum("erf,edf->erd", hidden, down_piece, preferred_element_type=jnp.float32)
    expert_rows = expert_sum.astype(jnp.bfloat16)
    returned = lax.all_to_all(expert_rows, "ep", split_axis=1, concat_axis=0, tiled=True)
    returned_rows = returned.reshape(EXPERTS * CAP, returned.shape[2])
    combined = jnp.zeros((normed.shape[0], normed.shape[1]), jnp.float32)
    for route_index in range(TOP):
        picking = (slots[:, route_index][:, None] == slot_index[None, :]).astype(jnp.bfloat16)
        chosen_rows = jnp.dot(picking, returned_rows, preferred_element_type=jnp.float32)
        combined = combined + route_weight[:, route_index : route_index + 1] * chosen_rows
    moe_out = combined.astype(jnp.bfloat16)
    return (mixed_out, moe_out)


def solution(mesh):
    return jax.shard_map(
        body,
        mesh=mesh,
        in_specs=(
            P("ep", "tp"),
            P("tp"),
            P("tp", None),
            P(("ep", "tp"), None),
            P(),
            P(("ep", "tp"), None),
            P(("ep", "tp"), None),
            P("ep", None, "tp"),
            P("ep", None, "tp"),
            P("ep", None, "tp"),
        ),
        out_specs=(P(("ep", "tp"), None), P(("ep", "tp"), None)),
        check_vma=False,
    )
```

profile of v0, /device:TPU:0, one launch (start us, length us, event | category | flops | bytes accessed | tf_op | source)
XLA Modules:
  0.0 554.3 jit_solution(15557223583954882724)
XLA Ops:
  7.2 0.0 copy-start.5
  7.2 0.0 all-gather.7.cloned.1.call-start
  7.2 0.7 all-gather.7.cloned.1.call-update
  7.9 0.0 all-gather.11.cloned.1.call-start
  8.0 0.7 all-gather.11.cloned.1.call-update
  8.7 0.0 all-gather.9.cloned.1.call-start
  8.7 0.7 all-gather.9.cloned.1.call-update
  9.4 0.1 copy.47
  9.6 0.1 eq.138
  9.7 0.1 eq.134
  9.9 1.2 reduce-window.6
  11.0 0.2 slice_reduce_fusion
  11.3 0.1 fusion.23
  11.4 0.1 reduce_sum.21
  11.5 0.1 copy.50
  11.6 0.3 fusion.2
  11.9 0.0 copy-done.4
  12.0 2.8 convolution_convert_fusion
  14.7 5.3 all-to-all-start.1
  20.1 0.0 copy-done.3
  20.1 3.9 collective-permute-start
  24.0 0.0 all-gather.5.cloned.1.call-update
  24.1 30.0 %collective-permute-done = bf16[15,128]{1,0:T(8,128)(2,1)S(1)} collective-permute-done((bf16[15,128]{1,0:T(8,128)(2,1)S(1)}, bf16[15,128]{1,0:T(8,128)(2,1)S(1)}, u32[]{:S(2)}, u32[]{:S(2)}) %collective-permute-start) | collective-permute-done | bytes 3872 | tf_op jit(solution)/shard_map/ppermute | solution.py:16
  54.1 0.1 maximum_convert_fusion
  54.2 0.1 slice_add_fusion.1
  54.2 0.1 slice_add_fusion
  54.3 0.1 slice_add_fusion.2
  54.4 1.1 fusion.12
  55.4 0.8 all-to-all-done.1
  56.2 5.2 all-to-all-start
  61.4 1.9 copy.51
  63.3 107.9 %all-gather.7.cloned.1.call-done = bf16[4,2048,1024]{2,1,0:T(8,128)(2,1)} async-done(((bf16[4,2048,128]{2,1,0:T(8,128)(2,1)}), bf16[4,2048,1024]{2,1,0:T(8,128)(2,1)}) %all-gather.7.cloned.1.call-update) | async-done | bytes 16777232 | tf_op jit(solution)/shard_map/all_gather | solution.py:88
  171.2 11.9 %fusion.28 = f32[4,192,1024]{2,1,0:T(8,128)} fusion(bf16[4,192,2048]{2,1,0:T(8,128)(2,1)} %bitcast.48, bf16[4,2048,1024]{2,1,0:T(8,128)(2,1)} %all-gather.7.cloned.1.call-done), kind=kOutput, calls=%fused_computation.62 | convolution fusion | flops 3221225472 | bytes 23068672 | tf_op jit(solution)/shard_map/erd,edf->erf/dot_general | solution.py:91
  183.2 142.6 %all-gather.11.cloned.1.call-done = bf16[4,2048,1024]{2,1,0:T(8,128)(2,1)} async-done(((bf16[4,2048,128]{2,1,0:T(8,128)(2,1)}), bf16[4,2048,1024]{2,1,0:T(8,128)(2,1)}) %all-gather.11.cloned.1.call-update) | async-done | bytes 16777232 | tf_op jit(solution)/shard_map/all_gather | solution.py:90
  325.8 151.6 %all-gather.9.cloned.1.call-done = bf16[4,2048,1024]{2,1,0:T(8,128)(2,1)} async-done(((bf16[4,2048,128]{2,1,0:T(8,128)(2,1)}), bf16[4,2048,1024]{2,1,0:T(8,128)(2,1)}) %all-gather.9.cloned.1.call-update) | async-done | bytes 16777232 | tf_op jit(solution)/shard_map/all_gather | solution.py:89
  477.4 17.7 %convolution_convert_fusion.1 = bf16[4,192,2048]{2,1,0:T(8,128)(2,1)} fusion(bf16[4,2048,1024]{2,1,0:T(8,128)(2,1)} %all-gather.11.cloned.1.call-done, f32[4,192,1024]{2,1,0:T(8,128)} %fusion.28, bf16[4,192,2048]{2,1,0:T(8,128)(2,1)S(1)} %bitcast.49, bf16[4,2048,1024]{2,1,0:T(8,128)(2,1)} %all-gather.9.cloned.1.call-done), kind=kOutput, calls=%fused_computation.1 | convolution fusion | flops 6448742400 | bytes 42991616 | tf_op jit(solution)/shard_map/erf,edf->erd/dot_general | solution.py:94
  495.1 6.0 %copy.52 = bf16[4,192,2048]{2,0,1:T(4,128)(2,1)} copy(bf16[4,192,2048]{2,1,0:T(8,128)(2,1)} %convolution_convert_fusion.1) | data formatting | bytes 6291456 | tf_op jit(solution)/shard_map/convert_element_type | solution.py:95
  501.1 0.0 all-to-all-done
  501.1 0.7 copy-done.2
  501.8 3.9 all-to-all-start.2
  505.7 1.1 copy.46
  506.9 17.0 %all-gather.5.cloned.1.call-done = bf16[1024,2048]{1,0:T(8,128)(2,1)} async-done(((bf16[128,2048]{1,0:T(8,128)(2,1)}), bf16[1024,2048]{1,0:T(8,128)(2,1)}) %all-gather.5.cloned.1.call-update) | async-done | bytes 4194320 | tf_op jit(solution)/shard_map/all_gather | solution.py:73
  523.9 3.7 convolution_convert_fusion.2
  527.6 14.8 %all-to-all-done.2 = bf16[4,192,2048]{2,0,1:T(4,128)(2,1)S(1)} async-done(((bf16[4,192,2048]{2,0,1:T(4,128)(2,1)}), bf16[4,192,2048]{2,0,1:T(4,128)(2,1)S(1)}, u32[]{:S(2)}, u32[]{:S(2)}) %all-to-all-start.2) | async-done | bytes 3145760 | tf_op jit(solution)/shard_map/all_to_all | solution.py:96
  542.5 1.7 copy.53
  544.2 0.4 copy.54
  544.6 1.0 convolution_multiply_fusion.1
  545.7 2.1 fusion.1
  (25 shorter events, 0.1 us)
Async XLA Ops:
  7.2 2.3 copy-start.5
  7.2 4.4 copy-start.1
  7.2 164.1 %all-gather.7.cloned.1.call-start = ((), (), s32[]{:S(2)}) async-start(), calls=%async_computation.4 | async-start | bytes 18874368 | tf_op jit(solution)/shard_map/all_gather | solution.py:88
  7.9 4.0 copy-start.4
  7.9 317.8 %all-gather.11.cloned.1.call-start = ((), (), s32[]{:S(2)}) async-start(), calls=%async_computation.6 | async-start | bytes 18874368 | tf_op jit(solution)/shard_map/all_gather | solution.py:90
  8.7 468.7 %all-gather.9.cloned.1.call-start = ((), (), s32[]{:S(2)}) async-start(), calls=%async_computation.5 | async-start | bytes 18874368 | tf_op jit(solution)/shard_map/all_gather | solution.py:89
  14.7 5.3 copy-start.3
  14.7 41.5 %all-to-all-start.1 = ((bf16[16,48,2048]{2,1,0:T(8,128)(2,1)}), bf16[16,48,2048]{2,1,0:T(8,128)(2,1)S(1)}, u32[]{:S(2)}, u32[]{:S(2)}) async-start(bf16[16,48,2048]{2,1,0:T(8,128)(2,1)} %bitcast.7), calls=%async_computation.1 | async-start | bytes 6291456 | tf_op jit(solution)/shard_map/all_to_all | solution.py:87
  20.0 34.3 %copy-start.7 = (f32[128]{0:T(128)S(1)}, f32[128]{0:T(128)}, u32[]{:S(2)}) copy-start(f32[128]{0:T(128)} %param.11) | copy-start | bytes 1540
  20.0 503.9 %all-gather.5.cloned.1.call-start = ((), (), s32[]{:S(2)}) async-start(), calls=%async_computation.3 | async-start | bytes 4718592 | tf_op jit(solution)/shard_map/all_gather | solution.py:73
  20.1 34.0 %collective-permute-start = (bf16[15,128]{1,0:T(8,128)(2,1)S(1)}, bf16[15,128]{1,0:T(8,128)(2,1)S(1)}, u32[]{:S(2)}, u32[]{:S(2)}) collective-permute-start(bf16[15,128]{1,0:T(8,128)(2,1)S(1)} %slice.57), channel_id=1, source_target_pairs={{0,8},{8,16},{16,24},{1,9},{9,17},{17,25},{2,10},{10,18},{18,26},{... | collective-permute-start | bytes 11528 | tf_op jit(solution)/shard_map/ppermute | solution.py:16
  56.2 444.9 %all-to-all-start = ((bf16[8,128,128]{2,1,0:T(8,128)(2,1)}), bf16[8,128,128]{2,1,0:T(8,128)(2,1)S(1)}, u32[]{:S(2)}, u32[]{:S(2)}) async-start(bf16[8,128,128]{2,1,0:T(8,128)(2,1)} %bitcast), calls=%async_computation | async-start | bytes 524288 | tf_op jit(solution)/shard_map/all_to_all | solution.py:70
  171.2 306.1 %copy-start = (bf16[4,4,48,2048]{3,2,0,1:T(8,128)(2,1)S(1)}, bf16[4,4,48,2048]{3,2,0,1:T(8,128)(2,1)}, u32[]{:S(2)}) copy-start(bf16[4,4,48,2048]{3,2,0,1:T(8,128)(2,1)} %copy.51) | copy-start | bytes 9437188
  501.1 4.6 copy-start.6
  501.1 0.7 copy-start.2
  501.8 40.6 %all-to-all-start.2 = ((bf16[4,192,2048]{2,0,1:T(4,128)(2,1)}), bf16[4,192,2048]{2,0,1:T(4,128)(2,1)S(1)}, u32[]{:S(2)}, u32[]{:S(2)}) async-start(bf16[4,192,2048]{2,0,1:T(4,128)(2,1)} %copy.52), calls=%async_computation.2 | async-start | bytes 6291456 | tf_op jit(solution)/shard_map/all_to_all | solution.py:96
Sparse Core Ops, SparseCore 0:
  9.6 161.6 all-gather.6
  172.8 152.8 all-gather.10
  327.4 149.9 all-gather.8
  478.8 45.0 all-gather.4
where the time goes:
time: 555 us; the launch traced here: 554 us
  waiting for transfers between devices  467 us (84%)
  matrix products  39.2 us (7%)
  starting transfers between devices  18.4 us (3%)
  between operations  14 us (3%)
  local copies, waits for them, and re-layouts  12.8 us (2%)
    all_gather x1, waiting for transfers between devices, body(): up_piece = lax.all_gather(up_weight, 'tp', axis=2, tiled=True)  152 us
    all_gather x1, waiting for transfers between devices, body(): down_piece = lax.all_gather(down_weight, 'tp', axis=2, tiled=True)  143 us
    all_gather x1, waiting for transfers between devices, body(): gate_piece = lax.all_gather(gate_weight, 'tp', axis=2, tiled=True)  108 us
    ppermute x1, waiting for transfers between devices, from_behind(): return lax.ppermute(shard, axis, pairs)  30 us
    dot_general x1, matrix products, body(): jnp.einsum('erf,edf->erd', hidden, down_piece, preferred_element_type=jnp...  17.7 us
    all_gather x1, waiting for transfers between devices, body(): lax.all_gather(mix_weight, 'tp', axis=0, tiled=True)  17 us
    all_to_all x1, waiting for transfers between devices, body(): lax.all_to_all(expert_rows, 'ep', split_axis=1, concat_axis=0, tiled=True)  14.8 us
    dot_general x1, matrix products, body(): jnp.einsum('erd,edf->erf', arrived, gate_piece, preferred_element_type=jn...  11.9 us
  transfers between devices with their start and end apart: 8, of which 7 were waited for; matrix products, arithmetic and copies ran while one was open for 9% of the time, Pallas kernels for 0%

commit v1 on v0

--- a/solution.py
+++ b/solution.py
@@ -8,6 +8,12 @@
 TOP = 2
 CAP = 48
 eps_norm = 1e-06
+
+
+def joined_along(blocks, dim):
+    shape = list(blocks.shape[1:])
+    shape[dim] *= blocks.shape[0]
+    return jnp.moveaxis(blocks, 0, dim).reshape(shape)
 
 
 def from_behind(shard, axis, by):
@@ -86,10 +92,28 @@
     outgoing = outgoing.reshape(EXPERTS, CAP, normed.shape[1])
     arrived = lax.all_to_all(outgoing, "ep", split_axis=0, concat_axis=1, tiled=True)
     gate_piece = lax.all_gather(gate_weight, "tp", axis=2, tiled=True)
-    up_piece = lax.all_gather(up_weight, "tp", axis=2, tiled=True)
     down_piece = lax.all_gather(down_weight, "tp", axis=2, tiled=True)
     gate_part = jnp.einsum("erd,edf->erf", arrived, gate_piece, preferred_element_type=jnp.float32)
-    upward = jnp.einsum("erd,edf->erf", arrived, up_piece, preferred_element_type=jnp.float32)
+    size, position_2, width = (lax.axis_size("tp"), lax.axis_index("tp"), up_weight.shape[2])
+    right = [(i_2, (i_2 + 1) % size) for i_2 in range(size)]
+    backward = [(i_2, (i_2 - 1) % size) for i_2 in range(size)]
+    half = size // 2
+    blocks = {}
+    from_left = from_right = up_weight
+    for step in range(half + 1):
+        next_left = lax.ppermute(from_left, "tp", right) if step < half else None
+        next_right = lax.ppermute(from_right, "tp", backward) if step < size - half - 1 else None
+        blocks[-step] = jnp.einsum(
+            "erd,edf->erf", arrived, from_left, preferred_element_type=jnp.float32
+        )
+        if 0 < step < size - half:
+            blocks[step] = jnp.einsum(
+                "erd,edf->erf", arrived, from_right, preferred_element_type=jnp.float32
+            )
+        from_left, from_right = (next_left, next_right)
+    blocks = jnp.stack([blocks[k] for k in sorted(blocks)])
+    blocks = blocks[(jnp.arange(size) - position_2 + half) % size]
+    upward = joined_along(blocks, 2)
     hidden = (jax.nn.silu(gate_part) * upward).astype(jnp.bfloat16)
     expert_sum = jnp.einsum("erf,edf->erd", hidden, down_piece, preferred_element_type=jnp.float32)
     expert_rows = expert_sum.astype(jnp.bfloat16)

time: 555 us -> 536 us (0.966)
  waiting for transfers between devices: 467 us -> 377 us
  starting transfers between devices: 18.4 us -> 73.9 us
  matrix products: 39.2 us -> 51.1 us
    ppermute x0 -> x7, waiting for transfers between devices: none -> 241 us  [the longest x4 203 us: body(): next_left = lax.ppermute(from_left, 'tp', right) if step < half else None]
    all_gather x1 -> x0, waiting for transfers between devices: 152 us -> none  [body(): up_piece = lax.all_gather(up_weight, 'tp', axis=2, tiled=True)]
    all_gather x1, waiting for transfers between devices: 108 us -> 0.01 us  [body(): gate_piece = lax.all_gather(gate_weight, 'tp', axis=2, tiled=True)]
    all_gather x1, waiting for transfers between devices: 143 us -> 102 us  [body(): down_piece = lax.all_gather(down_weight, 'tp', axis=2, tiled=True)]
    ppermute x0 -> x7, starting transfers between devices: none -> 36 us  [the longest x4 30.2 us: body(): next_left = lax.ppermute(from_left, 'tp', right) if step < half else None]
    ppermute x1, waiting for transfers between devices: 30 us -> 0.01 us  [from_behind(): return lax.ppermute(shard, axis, pairs)]
    all_to_all x1, starting transfers between devices: 5.19 us -> 26.5 us  [body(): lax.all_to_all(pooled, 'tp', split_axis=0, concat_axis=1, tiled=True)]
    dot_general x1 -> x8, matrix products: 11.9 us -> 23.7 us  [the longest x5 15.2 us: body(): jnp.einsum('erd,edf->erf', arrived, from_left, preferred_element_type=jnp...]
  transfers between devices with their start and end apart: 8 -> 14, of which waited for: 7 -> 8; matrix products, arithmetic and copies ran while one was open for 9% -> 12% of each run, Pallas kernels for 0% -> 0%
where the time goes in v1:
time: 536 us; the launch traced here: 534 us
  waiting for transfers between devices  377 us (70%)
  starting transfers between devices  73.9 us (14%)
  matrix products  51.1 us (10%)
  local copies, waits for them, and re-layouts  15.7 us (3%)
  between operations  14 us (3%)
    ppermute x4, waiting for transfers between devices, body(): next_left = lax.ppermute(from_left, 'tp', right) if step < half else None  203 us
    all_gather x1, waiting for transfers between devices, body(): down_piece = lax.all_gather(down_weight, 'tp', axis=2, tiled=True)  102 us
    ppermute x3, waiting for transfers between devices, body(): lax.ppermute(from_right, 'tp', backward)  38.4 us
    ppermute x4, starting transfers between devices, body(): next_left = lax.ppermute(from_left, 'tp', right) if step < half else None  30.2 us
    all_to_all x1, starting transfers between devices, body(): lax.all_to_all(pooled, 'tp', split_axis=0, concat_axis=1, tiled=True)  26.5 us
    all_gather x1, waiting for transfers between devices, body(): lax.all_gather(mix_weight, 'tp', axis=0, tiled=True)  21.5 us
    dot_general x1, matrix products, body(): jnp.einsum('erf,edf->erd', hidden, down_piece, preferred_element_type=jnp...  17.8 us
    dot_general x5, matrix products, body(): jnp.einsum('erd,edf->erf', arrived, from_left, preferred_element_type=jnp...  15.2 us
  transfers between devices with their start and end apart: 14, of which 8 were waited for; matrix products, arithmetic and copies ran while one was open for 12% of the time, Pallas kernels for 0%

profile of v1, /device:TPU:0, one launch (start us, length us, event | category | flops | bytes accessed | tf_op | source)
XLA Modules:
  0.0 534.3 jit_solution(13503935739335874954)
XLA Ops:
  7.2 0.7 all-gather.6.cloned.1.call-update
  8.0 0.7 all-gather.8.cloned.1.call-update
  8.7 0.5 collective-permute-start.1
  9.2 49.7 %collective-permute-done.1 = bf16[4,2048,128]{2,1,0:T(8,128)(2,1)S(1)} collective-permute-done((bf16[4,2048,128]{2,1,0:T(8,128)(2,1)}, bf16[4,2048,128]{2,1,0:T(8,128)(2,1)S(1)}, u32[]{:S(2)}, u32[]{:S(2)}) %collective-permute-start.1) | collective-permute-done | bytes 2097184 | tf_op jit(solution)/shard_map/ppermute | solution.py:104
  58.9 1.6 collective-permute-start.2
  60.5 2.0 collective-permute-start.5
  62.5 0.1 copy.52
  62.6 0.1 eq.140
  62.8 0.1 eq.136
  62.9 79.9 %collective-permute-done.2 = bf16[4,2048,128]{2,1,0:T(8,128)(2,1)} collective-permute-done((bf16[4,2048,128]{2,1,0:T(8,128)(2,1)S(1)}, bf16[4,2048,128]{2,1,0:T(8,128)(2,1)}, u32[]{:S(2)}, u32[]{:S(2)}) %collective-permute-start.2) | collective-permute-done | bytes 2097184 | tf_op jit(solution)/shard_map/ppermute | solution.py:104
  142.8 10.4 %collective-permute-start.3 = (bf16[4,2048,128]{2,1,0:T(8,128)(2,1)}, bf16[4,2048,128]{2,1,0:T(8,128)(2,1)}, u32[]{:S(2)}, u32[]{:S(2)}) collective-permute-start(bf16[4,2048,128]{2,1,0:T(8,128)(2,1)} %collective-permute-done.2), channel_id=1, source_target_pairs={{0,1},{1,2},{2,3},{3,4},{4,5},{5,6},{6,7},{7,0},{8,9},{9,10},{10,1... | collective-permute-start | bytes 6291464 | tf_op jit(solution)/shard_map/ppermute | solution.py:104
  153.3 1.1 reduce-window.6
  154.4 0.2 slice_reduce_fusion
  154.8 0.1 reduce_sum.21
  155.0 0.3 fusion.3
  155.3 2.7 convolution_convert_fusion
  158.1 3.8 all-to-all-start.1
  162.0 3.8 collective-permute-start
  166.0 59.4 %collective-permute-done.3 = bf16[4,2048,128]{2,1,0:T(8,128)(2,1)} collective-permute-done((bf16[4,2048,128]{2,1,0:T(8,128)(2,1)}, bf16[4,2048,128]{2,1,0:T(8,128)(2,1)}, u32[]{:S(2)}, u32[]{:S(2)}) %collective-permute-start.3) | collective-permute-done | bytes 2097184 | tf_op jit(solution)/shard_map/ppermute | solution.py:104
  225.5 17.6 %collective-permute-start.4 = (bf16[4,2048,128]{2,1,0:T(8,128)(2,1)}, bf16[4,2048,128]{2,1,0:T(8,128)(2,1)}, u32[]{:S(2)}, u32[]{:S(2)}) collective-permute-start(bf16[4,2048,128]{2,1,0:T(8,128)(2,1)} %collective-permute-done.3), channel_id=1, source_target_pairs={{0,1},{1,2},{2,3},{3,4},{4,5},{5,6},{6,7},{7,0},{8,9},{9,10},{10,1... | collective-permute-start | bytes 6291464 | tf_op jit(solution)/shard_map/ppermute | solution.py:104
  243.4 1.1 fusion.22
  244.5 26.5 %all-to-all-start = ((bf16[8,128,128]{2,1,0:T(8,128)(2,1)}), bf16[8,128,128]{2,1,0:T(8,128)(2,1)S(1)}, u32[]{:S(2)}, u32[]{:S(2)}) async-start(bf16[8,128,128]{2,1,0:T(8,128)(2,1)} %bitcast), calls=%async_computation | async-start | bytes 524288 | tf_op jit(solution)/shard_map/all_to_all | solution.py:76
  270.9 0.2 copy.56
  271.2 3.8 collective-permute-start.7
  274.9 13.8 %collective-permute-done.4 = bf16[4,2048,128]{2,1,0:T(8,128)(2,1)} collective-permute-done((bf16[4,2048,128]{2,1,0:T(8,128)(2,1)}, bf16[4,2048,128]{2,1,0:T(8,128)(2,1)}, u32[]{:S(2)}, u32[]{:S(2)}) %collective-permute-start.4) | collective-permute-done | bytes 2097184 | tf_op jit(solution)/shard_map/ppermute | solution.py:104
  288.8 3.3 fusion.15
  292.1 3.3 fusion.14
  295.5 3.5 fusion.13
  298.9 1.8 fusion.12
  300.7 3.3 fusion.11
  304.0 3.3 fusion.10
  307.3 3.3 fusion.9
  310.7 38.4 %collective-permute-done.7 = bf16[4,2048,128]{2,1,0:T(8,128)(2,1)S(1)} collective-permute-done((bf16[4,2048,128]{2,1,0:T(8,128)(2,1)}, bf16[4,2048,128]{2,1,0:T(8,128)(2,1)S(1)}, u32[]{:S(2)}, u32[]{:S(2)}) %collective-permute-start.7) | collective-permute-done | bytes 2097184 | tf_op jit(solution)/shard_map/ppermute | solution.py:105
  349.1 1.8 fusion.8
  350.9 4.6 gather_fusion
  355.5 102.1 %all-gather.8.cloned.1.call-done = bf16[4,2048,1024]{2,1,0:T(8,128)(2,1)} async-done(((bf16[4,2048,128]{2,1,0:T(8,128)(2,1)}), bf16[4,2048,1024]{2,1,0:T(8,128)(2,1)}) %all-gather.8.cloned.1.call-update) | async-done | bytes 16777232 | tf_op jit(solution)/shard_map/all_gather | solution.py:95
  457.6 17.8 %convolution_convert_fusion.1 = bf16[4,192,2048]{2,1,0:T(8,128)(2,1)} fusion(bf16[4,2048,1024]{2,1,0:T(8,128)(2,1)} %all-gather.8.cloned.1.call-done, bf16[4,192,2048]{2,1,0:T(8,128)(2,1)S(1)} %bitcast.114, bf16[4,2048,1024]{2,1,0:T(8,128)(2,1)} %all-gather.6.cloned.1.call-done, f32[8,4,192,128]{3,2,1,0:T(8,128)} %gather_fusion), kind=kOutput, calls=%fused_computation.2 | convolution fusion | flops 6448742400 | bytes 42991616 | tf_op jit(solution)/shard_map/erf,edf->erd/dot_general | solution.py:118
  475.4 6.0 %copy.58 = bf16[4,192,2048]{2,0,1:T(4,128)(2,1)} copy(bf16[4,192,2048]{2,1,0:T(8,128)(2,1)} %convolution_convert_fusion.1) | data formatting | bytes 6291456 | tf_op jit(solution)/shard_map/convert_element_type | solution.py:119
  481.3 0.7 copy-done.3
  482.0 3.7 all-to-all-start.2
  485.7 1.1 copy.51
  486.9 21.5 %all-gather.4.cloned.1.call-done = bf16[1024,2048]{1,0:T(8,128)(2,1)} async-done(((bf16[128,2048]{1,0:T(8,128)(2,1)}), bf16[1024,2048]{1,0:T(8,128)(2,1)}) %all-gather.4.cloned.1.call-update) | async-done | bytes 4194320 | tf_op jit(solution)/shard_map/all_gather | solution.py:79
  508.4 3.7 convolution_convert_fusion.2
  512.1 10.4 %all-to-all-done.2 = bf16[4,192,2048]{2,0,1:T(4,128)(2,1)S(1)} async-done(((bf16[4,192,2048]{2,0,1:T(4,128)(2,1)}), bf16[4,192,2048]{2,0,1:T(4,128)(2,1)S(1)}, u32[]{:S(2)}, u32[]{:S(2)}) %all-to-all-start.2) | async-done | bytes 3145760 | tf_op jit(solution)/shard_map/all_to_all | solution.py:120
  522.5 1.7 copy.59
  524.2 0.4 copy.60
  524.6 1.0 convolution_multiply_fusion.1
  525.7 2.1 fusion.2
  (52 shorter events, 0.8 us)
Async XLA Ops:
  7.2 55.3 %copy-start.6 = (s32[256,2]{0,1:T(2,128)S(1)}, s32[256,2]{0,1:T(2,128)}, u32[]{:S(2)}) copy-start(s32[256,2]{0,1:T(2,128)} %param.15) | copy-start | bytes 6148
  7.2 147.8 %copy-start = (bf16[256,2048]{1,0:T(8,128)(2,1)S(1)}, bf16[256,2048]{1,0:T(8,128)(2,1)}, u32[]{:S(2)}) copy-start(bf16[256,2048]{1,0:T(8,128)(2,1)} %param.13) | copy-start | bytes 3145732
  7.2 148.2 %copy-start.5 = (f32[2048]{0:T(1024)S(1)}, f32[2048]{0:T(1024)}, u32[]{:S(2)}) copy-start(f32[2048]{0:T(1024)} %param.14) | copy-start | bytes 24580
  7.2 348.3 %all-gather.6.cloned.1.call-start = ((), (), s32[]{:S(2)}) async-start(), calls=%async_computation.4 | async-start | bytes 18874368 | tf_op jit(solution)/shard_map/all_gather | solution.py:94
  7.9 449.6 %all-gather.8.cloned.1.call-start = ((), (), s32[]{:S(2)}) async-start(), calls=%async_computation.5 | async-start | bytes 18874368 | tf_op jit(solution)/shard_map/all_gather | solution.py:95
  8.7 50.3 %collective-permute-start.1 = (bf16[4,2048,128]{2,1,0:T(8,128)(2,1)}, bf16[4,2048,128]{2,1,0:T(8,128)(2,1)S(1)}, u32[]{:S(2)}, u32[]{:S(2)}) collective-permute-start(bf16[4,2048,128]{2,1,0:T(8,128)(2,1)} %param.18), channel_id=1, source_target_pairs={{0,1},{1,2},{2,3},{3,4},{4,5},{5,6},{6,7},{7,0},{8,9},{9,10},{10,1... | collective-permute-start | bytes 6291464 | tf_op jit(solution)/shard_map/ppermute | solution.py:104
  58.9 99.2 %copy-start.9 = (bf16[4,2048,128]{2,1,0:T(8,128)(2,1)}, bf16[4,2048,128]{2,1,0:T(8,128)(2,1)S(1)}, u32[]{:S(2)}) copy-start(bf16[4,2048,128]{2,1,0:T(8,128)(2,1)S(1)} %collective-permute-done.1) | copy-start | bytes 6291460
  58.9 83.9 %collective-permute-start.2 = (bf16[4,2048,128]{2,1,0:T(8,128)(2,1)S(1)}, bf16[4,2048,128]{2,1,0:T(8,128)(2,1)}, u32[]{:S(2)}, u32[]{:S(2)}) collective-permute-start(bf16[4,2048,128]{2,1,0:T(8,128)(2,1)S(1)} %collective-permute-done.1), channel_id=1, source_target_pairs={{0,1},{1,2},{2,3},{3,4},{4,5},{5,6},{6,7},{7,0},{8,9},{9,10},{10,1... | collective-permute-start | bytes 6291464 | tf_op jit(solution)/shard_map/ppermute | solution.py:104
  60.5 105.5 %collective-permute-start.5 = (bf16[4,2048,128]{2,1,0:T(8,128)(2,1)}, bf16[4,2048,128]{2,1,0:T(8,128)(2,1)}, u32[]{:S(2)}, u32[]{:S(2)}) collective-permute-start(bf16[4,2048,128]{2,1,0:T(8,128)(2,1)} %param.18), channel_id=1, source_target_pairs={{0,7},{1,0},{2,1},{3,2},{4,3},{5,4},{6,5},{7,6},{8,15},{9,8},{10,9... | collective-permute-start | bytes 6291464 | tf_op jit(solution)/shard_map/ppermute | solution.py:105
  142.8 82.7 %collective-permute-start.3 = (bf16[4,2048,128]{2,1,0:T(8,128)(2,1)}, bf16[4,2048,128]{2,1,0:T(8,128)(2,1)}, u32[]{:S(2)}, u32[]{:S(2)}) collective-permute-start(bf16[4,2048,128]{2,1,0:T(8,128)(2,1)} %collective-permute-done.2), channel_id=1, source_target_pairs={{0,1},{1,2},{2,3},{3,4},{4,5},{5,6},{6,7},{7,0},{8,9},{9,10},{10,1... | collective-permute-start | bytes 6291464 | tf_op jit(solution)/shard_map/ppermute | solution.py:104
  158.1 3.9 copy-start.4
  158.1 86.4 %all-to-all-start.1 = ((bf16[16,48,2048]{2,1,0:T(8,128)(2,1)}), bf16[16,48,2048]{2,1,0:T(8,128)(2,1)S(1)}, u32[]{:S(2)}, u32[]{:S(2)}) async-start(bf16[16,48,2048]{2,1,0:T(8,128)(2,1)} %bitcast.7), calls=%async_computation.1 | async-start | bytes 6291456 | tf_op jit(solution)/shard_map/all_to_all | solution.py:93
  161.9 81.4 %copy-start.8 = (f32[128]{0:T(128)S(1)}, f32[128]{0:T(128)}, u32[]{:S(2)}) copy-start(f32[128]{0:T(128)} %param.11) | copy-start | bytes 1540
  161.9 346.4 %all-gather.4.cloned.1.call-start = ((), (), s32[]{:S(2)}) async-start(), calls=%async_computation.3 | async-start | bytes 4718592 | tf_op jit(solution)/shard_map/all_gather | solution.py:79
  162.0 81.1 %collective-permute-start = (bf16[15,128]{1,0:T(8,128)(2,1)S(1)}, bf16[15,128]{1,0:T(8,128)(2,1)S(1)}, u32[]{:S(2)}, u32[]{:S(2)}) collective-permute-start(bf16[15,128]{1,0:T(8,128)(2,1)S(1)} %slice.57), channel_id=1, source_target_pairs={{0,8},{8,16},{16,24},{1,9},{9,17},{17,25},{2,10},{10,18},{18,26},{... | collective-permute-start | bytes 11528 | tf_op jit(solution)/shard_map/ppermute | solution.py:22
  166.0 105.2 %collective-permute-start.6 = (bf16[4,2048,128]{2,1,0:T(8,128)(2,1)}, bf16[4,2048,128]{2,1,0:T(8,128)(2,1)}, u32[]{:S(2)}, u32[]{:S(2)}) collective-permute-start(bf16[4,2048,128]{2,1,0:T(8,128)(2,1)} %collective-permute-done.5), channel_id=1, source_target_pairs={{0,7},{1,0},{2,1},{3,2},{4,3},{5,4},{6,5},{7,6},{8,15},{9,8},{10,9... | collective-permute-start | bytes 6291464 | tf_op jit(solution)/shard_map/ppermute | solution.py:105
  225.5 63.3 %collective-permute-start.4 = (bf16[4,2048,128]{2,1,0:T(8,128)(2,1)}, bf16[4,2048,128]{2,1,0:T(8,128)(2,1)}, u32[]{:S(2)}, u32[]{:S(2)}) collective-permute-start(bf16[4,2048,128]{2,1,0:T(8,128)(2,1)} %collective-permute-done.3), channel_id=1, source_target_pairs={{0,1},{1,2},{2,3},{3,4},{4,5},{5,6},{6,7},{7,0},{8,9},{9,10},{10,1... | collective-permute-start | bytes 6291464 | tf_op jit(solution)/shard_map/ppermute | solution.py:104
  244.5 236.9 %all-to-all-start = ((bf16[8,128,128]{2,1,0:T(8,128)(2,1)}), bf16[8,128,128]{2,1,0:T(8,128)(2,1)S(1)}, u32[]{:S(2)}, u32[]{:S(2)}) async-start(bf16[8,128,128]{2,1,0:T(8,128)(2,1)} %bitcast), calls=%async_computation | async-start | bytes 524288 | tf_op jit(solution)/shard_map/all_to_all | solution.py:76
  271.1 78.0 %copy-start.1 = (bf16[4,4,48,2048]{3,2,0,1:T(8,128)(2,1)}, bf16[4,4,48,2048]{3,2,0,1:T(8,128)(2,1)S(1)}, u32[]{:S(2)}) copy-start(bf16[4,4,48,2048]{3,2,0,1:T(8,128)(2,1)S(1)} %copy.56) | copy-start | bytes 9437188
  271.2 78.0 %collective-permute-start.7 = (bf16[4,2048,128]{2,1,0:T(8,128)(2,1)}, bf16[4,2048,128]{2,1,0:T(8,128)(2,1)S(1)}, u32[]{:S(2)}, u32[]{:S(2)}) collective-permute-start(bf16[4,2048,128]{2,1,0:T(8,128)(2,1)} %collective-permute-done.6), channel_id=1, source_target_pairs={{0,7},{1,0},{2,1},{3,2},{4,3},{5,4},{6,5},{7,6},{8,15},{9,8},{10,9... | collective-permute-start | bytes 6291464 | tf_op jit(solution)/shard_map/ppermute | solution.py:105
  295.5 3.5 copy-start.10
  350.9 106.7 %copy-start.2 = (bf16[4,4,48,2048]{3,2,0,1:T(8,128)(2,1)S(1)}, bf16[4,4,48,2048]{3,2,0,1:T(8,128)(2,1)}, u32[]{:S(2)}) copy-start(bf16[4,4,48,2048]{3,2,0,1:T(8,128)(2,1)} %copy-done.1) | copy-start | bytes 9437188
  481.3 4.4 copy-start.7
  481.3 0.7 copy-start.3
  482.0 40.5 %all-to-all-start.2 = ((bf16[4,192,2048]{2,0,1:T(4,128)(2,1)}), bf16[4,192,2048]{2,0,1:T(4,128)(2,1)S(1)}, u32[]{:S(2)}, u32[]{:S(2)}) async-start(bf16[4,192,2048]{2,0,1:T(4,128)(2,1)} %copy.58), calls=%async_computation.2 | async-start | bytes 6291456 | tf_op jit(solution)/shard_map/all_to_all | solution.py:120
Sparse Core Ops, SparseCore 0:
  9.6 255.6 all-gather.5
  266.9 190.5 all-gather.7
  459.2 49.1 all-gather.3
